TPU v7x, 256 devices: a whole 4x4x8 slice. The times are simulated.
256 devices in a mesh: dp: 4 (over x), kv: 32 (over z, y), tp: 2 (over core).
Axes of the slice: x: 4, y: 4, z: 8, core: 2. Of those that a mesh axis runs over, the one named last changes fastest.
Arguments:
- tokens: bfloat16 [4, 8192, 1024], P('dp', 'kv', 'tp'), may hold values from -6 to 6
- norm_gain: float32 [1024], replicated, may hold values from 0.1 to 1.9
- w_query: bfloat16 [1024, 1024], P(None, 'tp'), may hold values from -0.1875 to 0.1875
- w_key: bfloat16 [1024, 256], P(None, 'tp'), may hold values from -0.1875 to 0.1875
- w_value: bfloat16 [1024, 256], P(None, 'tp'), may hold values from -0.1875 to 0.1875
- q_gain: float32 [64], replicated, may hold values from 0.1 to 1.9
- k_gain: float32 [64], replicated, may hold values from 0.1 to 1.9
- w_out: bfloat16 [1024, 1024], P('tp'), may hold values from -4 to 4
- chosen: int32 [4, 256, 16], P('dp', 'kv'), may hold values from -1 to 255, as said below
Outputs:
- mixed: bfloat16 [4, 8192, 1024], P('dp', 'kv', 'tp')
- log_total: float32 [4, 16, 8192], P('dp', 'tp', 'kv')
Inputs may be any that keep to these rules, and one draw needn't show every extreme that they name: Each row of chosen (one query block b) holds distinct key block numbers, all at most b, and -1 for empty entries; b itself is always present; a row is full (16 blocks) whenever at least 16 blocks may be chosen by it. Over the 8 rows of one index of kv, the chosen blocks that lie on any one other index of kv are at most 4 distinct ones, and exactly 4 of those on the index just before, for every index but the first. Some blocks are chosen far more often than others.
All inputs are finite; a program needn't handle non-finite values.
Results may differ from a plain program's by a relative error of at most 0.015.
Values may be sent and summed in bfloat16 or wider, within the bound.
A program may use at most 64 MiB of HBM per device.

v0:
```python
import functools
import math

import jax
import jax.numpy as jnp
from jax import lax
from jax.experimental import pallas as pl
from jax.experimental.pallas import tpu as pltpu
from jax.sharding import PartitionSpec as P

MESH = pl.DeviceIdType.MESH
F32 = jnp.float32
BF16 = jnp.bfloat16
I32 = jnp.int32

NZ, NY = 8, 4
NB = 8
BLK = 32
TOPB = 16
MOST = 4
HD = 64
HEADS = 8
TOK = NB * BLK
EPS = 1e-6
SEQ = 8192
OWN = NZ * NY * MOST
LANDED = OWN + NB
FAR = -1e30
PAIRS = ((0, 5), (2, 7), (1, 4), (3, 6))
NEAR = ((0, 1), (0, 2), (0, 3), (1, 0), (-1, 0), (2, 0), (-2, 0))
SERVED = ((0, 1), (0, 2), (0, 3), (2, 0), (-2, 0), (-1, 0))
CHUNKS = 4
STEP = TOK // CHUNKS
PIECES = 2
PER = NB // PIECES
LOG2E = math.log2(math.e)


def half_sums(x):
    row = lax.broadcasted_iota(I32, (128, 128), 0) // HD
    col = lax.broadcasted_iota(I32, (128, 128), 1) // HD
    ones = jnp.where(row == col, 1.0, 0.0).astype(BF16)
    high = x.astype(BF16)
    low = (x - high.astype(F32)).astype(BF16)
    return jnp.dot(high, ones, preferred_element_type=F32) + jnp.dot(
        low, ones, preferred_element_type=F32
    )


def head_norm(x, gain):
    return x * lax.rsqrt(half_sums(x * x) * (1.0 / HD) + EPS) * gain


def kernel(
    tokens, gain_h, wq, wk, wv, qg_h, kg_h, wo, chosen_h,
    out, logs,
    chosen, gain, qg, kg, tok, hid, wq_v, wkv_v, wo_v,
    c0, c1, c2, c3, c4, c5, c6, c7, p1, p2, p3,
    msg, land, sel_v, nsel_v, ent_v, sel_s, nsel_s, ent_s,
    upos, bias_t, bias_a, qbd, kvg, att, lsum, part, part_in,
    small_sem, load_sem, tab_sem, tok_send, tok_recv, nsel_send, nsel_recv,
    up_send, up_recv, dn_send, dn_recv, pln_send, pln_recv, y_send, y_recv, out_send, out_recv,
):
    dp = lax.axis_index("dp")
    kv = lax.axis_index("kv")
    tp = lax.axis_index("tp")
    z = kv // NY
    y = kv % NY
    col = (c0, c1, c2, c3, c4, c5, c6, c7)
    plane = (c0, p1, p2, p3)

    def dev(dz, dy):
        return (dp, ((z + dz) % NZ) * NY + (y + dy) % NY, tp)

    partner = (dp, kv, 1 - tp)

    def remote(src, dst, send, recv, where):
        return pltpu.make_async_remote_copy(
            src_ref=src, dst_ref=dst, send_sem=send, recv_sem=recv,
            device_id=where, device_id_type=MESH,
        )

    barrier = pltpu.get_barrier_semaphore()
    peers = [partner] + [dev(*at) for at in NEAR]
    for peer in peers:
        pl.semaphore_signal(barrier, inc=1, device_id=peer, device_id_type=MESH)

    small = [
        pltpu.make_async_copy(src, dst, small_sem.at[n])
        for n, (src, dst) in enumerate(
            ((chosen_h, chosen), (gain_h, gain), (qg_h, qg), (kg_h, kg))
        )
    ]
    for load in small:
        load.start()
    loads = [
        pltpu.make_async_copy(tokens, tok.at[tp], load_sem.at[0]),
        pltpu.make_async_copy(wk, wkv_v.at[:, pl.ds(0, 128)], load_sem.at[1]),
        pltpu.make_async_copy(wv, wkv_v.at[:, pl.ds(128, 128)], load_sem.at[2]),
        pltpu.make_async_copy(wq, wq_v, load_sem.at[3]),
    ]
    for p, pair in enumerate(PAIRS):
        for side in range(2):
            loads.append(
                pltpu.make_async_copy(
                    wo.at[pl.ds(pair[side] * HD, HD), :],
                    wo_v.at[pl.ds(p * 128 + side * HD, HD), :],
                    load_sem.at[4 + 2 * p + side],
                )
            )
    for load in loads:
        load.start()

    small[0].wait()
    ch = chosen[...]
    lane = lax.broadcasted_iota(I32, (NB, 256), 1)
    own_block = kv * NB + lax.broadcasted_iota(I32, (NB, 1), 0)
    member = jnp.zeros((NB, 256), I32)
    for e in range(TOPB):
        member = jnp.where(ch[:, e : e + 1] == lane, 1, member)
    present = jnp.broadcast_to(jnp.max(member, axis=0, keepdims=True), (NB, 256))
    inner = lane % NB
    rank = jnp.zeros((NB, 256), I32)
    for k in range(1, NB):
        rank = rank + jnp.where(inner >= k, pltpu.roll(present, k, 1), 0)
    sub = lax.broadcasted_iota(I32, (NB, 256), 0)
    sel = jnp.zeros((NB, 256), I32)
    for s in range(MOST):
        val = jnp.where((present == 1) & (rank == s), inner, 0)
        for k in (1, 2, 4):
            val = val + pltpu.roll(val, 256 - k, 1)
        sel = jnp.where(sub == s, val, sel)
    sel_v[...] = sel
    chip = lane // NB
    from_y = (y - chip % NY + NY) % NY
    from_z = (z - chip // NY + NZ) % NZ
    spot_of = jnp.where(
        chip == kv,
        OWN + inner,
        (from_y * NZ + from_z) * MOST + rank,
    )
    front = jnp.where(
        lax.broadcasted_iota(I32, (NB, TOPB), 1) == 0,
        own_block,
        jnp.where(ch == own_block, ch[:, 0:1], ch),
    )
    filled = jnp.where(front < 0, own_block, front)
    lane_e = lax.broadcasted_iota(I32, (NB, 128), 1)
    entry = jnp.zeros((NB, 128), I32)
    lane_u = lax.broadcasted_iota(I32, (NB, TOPB * BLK), 1)
    pos = jnp.full((NB, TOPB * BLK), FAR, F32)
    for e in range(TOPB):
        at = jnp.sum(jnp.where(filled[:, e : e + 1] == lane, spot_of, 0), axis=1, keepdims=True)
        entry = jnp.where(lane_e == e, at, entry)
        first = front[:, e : e + 1]
        pos = jnp.where(
            (lane_u // BLK == e) & (first >= 0),
            (first * BLK + lane_u % BLK).astype(F32),
            pos,
        )
    ent_v[...] = entry
    for r in range(NB):
        upos[r] = jnp.broadcast_to(pos[r : r + 1], (8, TOPB * BLK))

    rows = lax.broadcasted_iota(I32, (TOK, 128), 0)
    head_no = (tp * HEADS + rows // BLK + 1).astype(F32)
    bias_t[...] = (rows % BLK).astype(F32)
    bias_a[...] = jnp.exp2(head_no * (-8.0 / 16.0)) * (4.0 / SEQ * LOG2E)

    pl.semaphore_wait(barrier, len(peers))
    loads[0].wait()
    tok_copies = []
    for i in range(CHUNKS):
        at = pl.ds(i * STEP, STEP)
        c = remote(tok.at[tp, at], tok.at[tp, at], tok_send.at[i], tok_recv.at[i], partner)
        c.start()
        tok_copies.append(c)

    nsel_copies = []
    for n, (dz, dy) in enumerate(SERVED):
        c = remote(sel_v, nsel_v.at[n], nsel_send.at[n], nsel_recv.at[n], dev(-dz, -dy))
        c.start()
        nsel_copies.append(c)
    tabs = [
        pltpu.make_async_copy(sel_v, sel_s, tab_sem.at[0]),
        pltpu.make_async_copy(ent_v, ent_s, tab_sem.at[1]),
    ]
    for t in tabs:
        t.start()

    for load in small[1:]:
        load.wait()
    size = NB // CHUNKS

    def up(d, part):
        at = pl.ds(part * size, size)
        n = CHUNKS * d + part
        return remote(
            col[d].at[at], col[d + 1].at[at], up_send.at[n], up_recv.at[n], dev(1, 0)
        )

    def down(d, part):
        at = pl.ds(part * size, size)
        n = CHUNKS * d + part
        return remote(
            col[(8 - d) % 8].at[at], col[7 - d].at[at], dn_send.at[n], dn_recv.at[n], dev(-1, 0)
        )

    ups = [[up(d, bit) for bit in range(CHUNKS)] for d in range(4)]
    downs = [[down(d, bit) for bit in range(CHUNKS)] for d in range(3)]
    g0 = gain[:, 0:512]
    g1 = gain[:, 512:1024]
    kgain = jnp.concatenate([kg[...], kg[...]], axis=1)
    qgain = jnp.concatenate([qg[...], qg[...]], axis=1)
    loads[1].wait()
    loads[2].wait()
    plane_copies = []
    for i in range(CHUNKS):
        tok_copies[i].wait_recv()
        for half in range(2):
            at = pl.ds(i * STEP + half * (STEP // 2), STEP // 2)
            a = tok[0, at, :].astype(F32)
            b = tok[1, at, :].astype(F32)
            total = jnp.sum(a * a + b * b, axis=1, keepdims=True)
            r = lax.rsqrt(total * (1.0 / 1024.0) + EPS)
            hid[at, 0:512] = (a * r * g0).astype(BF16)
            hid[at, 512:1024] = (b * r * g1).astype(BF16)
        both = jnp.dot(hid[pl.ds(i * STEP, STEP), :], wkv_v[...], preferred_element_type=F32)
        keys = head_norm(both[:, 0:128], kgain).astype(BF16)
        values = both[:, 128:256].astype(BF16)
        for k, rows_of in enumerate((keys, values)):
            blocks = rows_of.reshape(size, BLK, 128)
            c0[pl.ds(i * size, size), :, 128 * k : 128 * (k + 1)] = blocks
            land[pl.ds(OWN + i * size, size), :, 128 * k : 128 * (k + 1)] = blocks
        ups[0][i].start()
        downs[0][i].start()
        for dy in (1, 3, 2):
            at = pl.ds(i * size, size)
            n = dy * CHUNKS + i
            c = remote(c0.at[at], plane[dy].at[at], pln_send.at[n], pln_recv.at[n], dev(0, dy))
            c.start()
            plane_copies.append(c)

    y_copies = {}

    def picked(table, source, d, dy, s):
        which = table[s, source * NB]
        return plane[dy][which] if d == 0 else col[d][which]

    def device_no(dz, dy):
        return ((z + dz + NZ) % NZ) * NY + (y + dy + NY) % NY

    def send(n, k, source, d, dy):
        for s in range(MOST):
            msg[k, s] = picked(nsel_s.at[n], source, d, dy, s)
        c = remote(
            msg.at[k], land.at[pl.ds(k * MOST, MOST)],
            y_send.at[k], y_recv.at[k], dev(*SERVED[n]),
        )
        c.start()
        y_copies[k] = c

    def serve(d):
        for n, dy in ((0, 1), (2, 3), (1, 2)):
            if not (d in (2, 6) and dy == 2):
                send(n, dy * NZ + d, device_no(-d, 0), d, 0)

    def keep(d, dy):
        for s in range(MOST):
            land[(dy * NZ + d) * MOST + s] = picked(sel_s, device_no(-d, -dy), d, dy, s)

    def turn(k):
        for bit in range(CHUNKS):
            ups[k - 1][bit].wait_recv()
            if k < 4:
                ups[k][bit].start()
                downs[k - 1][bit].wait_recv()
            if k < 3:
                downs[k][bit].start()

    for c in nsel_copies:
        c.wait_recv()
    ntab = [
        pltpu.make_async_copy(nsel_v.at[n], nsel_s.at[n], tab_sem.at[2 + n])
        for n in range(len(SERVED))
    ]
    for t in ntab:
        t.start()
    for t in tabs + ntab:
        t.wait()

    low_half = lax.broadcasted_iota(I32, (TOK, 128), 1) < HD

    def queries(one, two, pair, turned):
        flat = [
            jnp.dot(hid[...], wq_v[:, 128 * t : 128 * (t + 1)], preferred_element_type=F32)
            for t in (one, two)
        ]
        a, b = (head_norm(x, qgain) for x in flat)
        for (lo, hi), roll in ((pair, False), (turned, True)):
            if roll:
                a, b = pltpu.roll(a, HD, 1), pltpu.roll(b, HD, 1)
            first = jnp.where(low_half, a, 0.0).astype(BF16)
            second = jnp.where(low_half, 0.0, b).astype(BF16)
            for r in range(NB):
                qbd[r, pl.ds(lo * BLK, BLK), :] = first[r * BLK : (r + 1) * BLK]
                qbd[r, pl.ds(hi * BLK, BLK), :] = second[r * BLK : (r + 1) * BLK]

    turn(1)
    serve(1)
    keep(1, 0)
    keep(7, 0)
    loads[3].wait()
    queries(0, 2, PAIRS[0], PAIRS[2])
    turn(2)
    serve(2)
    serve(6)
    for c in plane_copies:
        c.wait_recv()
    for dy in (1, 2, 3):
        send(5, dy * NZ + 7, device_no(0, -dy), 0, dy)
    send(3, 2 * NZ + 2, device_no(0, -2), 0, 2)
    send(4, 2 * NZ + 6, device_no(0, -2), 0, 2)
    for dy in (1, 2, 3):
        keep(0, dy)
    keep(2, 0)
    keep(6, 0)
    queries(1, 3, PAIRS[1], PAIRS[3])
    turn(3)
    serve(3)
    serve(5)
    keep(3, 0)
    keep(5, 0)
    turn(4)
    serve(4)
    keep(4, 0)
    for load in loads[4:]:
        load.wait()
    for c in y_copies.values():
        c.wait_recv()

    def attend(r, carry):
        for e in range(TOPB):
            kvg[pl.ds(e * BLK, BLK), :] = land[ent_s[r, e]]
        raw = lax.dot_general(
            qbd[r], kvg[:, 0:128], (((1,), (1,)), ((), ())), preferred_element_type=F32
        )
        t = bias_t[...] + ((kv * NB + r) * BLK).astype(F32)
        a = bias_a[...]
        total = jnp.zeros((TOK, 128), F32)
        probs = []
        for i in range(4):
            u = upos[r, 0:1, 128 * i : 128 * (i + 1)]
            if i == 0:
                off = jnp.where(u > t, FAR, u - t)
            else:
                off = u - t
            w = jnp.exp2(raw[:, 128 * i : 128 * (i + 1)] * (LOG2E / 8.0) + a * off)
            total = total + w
            probs.append(w.astype(BF16))
        row_sum = jnp.sum(total, axis=1, keepdims=True)
        weighted = jnp.dot(
            jnp.concatenate(probs, axis=1), kvg[:, 128:256], preferred_element_type=F32
        )
        weighted = weighted / row_sum
        low = lax.broadcasted_iota(I32, (BLK, 128), 1) < HD
        for p, pair in enumerate(PAIRS):
            tile = jnp.where(
                low,
                weighted[pair[0] * BLK : (pair[0] + 1) * BLK],
                weighted[pair[1] * BLK : (pair[1] + 1) * BLK],
            )
            att[pl.ds(pl.multiple_of(r * BLK, BLK), BLK), 128 * p : 128 * (p + 1)] = tile.astype(
                BF16
            )
        lsum[r] = jnp.broadcast_to(row_sum, (TOK, 128))
        return carry

    def out_copy(piece):
        return remote(
            part.at[piece], part_in.at[piece], out_send.at[piece], out_recv.at[piece], partner
        )

    def do_piece(piece, carry):
        for r in range(PER):
            attend(piece * PER + r, 0)
        at = pl.ds(pl.multiple_of(piece * PER * BLK, PER * BLK), PER * BLK)
        theirs = pl.multiple_of((1 - tp) * 512, 512)
        part[piece] = jnp.dot(
            att[at, :], wo_v[:, pl.ds(theirs, 512)], preferred_element_type=F32
        ).astype(BF16)
        out_copy(piece).start()
        return carry

    lax.fori_loop(0, PIECES, do_piece, 0)
    out_copies = [out_copy(piece) for piece in range(PIECES)]
    lane_q = lax.broadcasted_iota(I32, (TOK, 128), 1)
    query = lax.broadcasted_iota(I32, (TOK, 128), 0) % BLK
    for side in range(2):
        sums = jnp.zeros((TOK, 128), F32)
        for r in range(4):
            sums = jnp.where(lane_q == r * BLK + query, lsum[4 * side + r], sums)
        logs[:, 128 * side : 128 * (side + 1)] = jnp.log(
            jnp.sum(sums.reshape(HEADS, BLK, 128), axis=1)
        )
    mine = pl.multiple_of(tp * 512, 512)
    for piece in range(PIECES):
        at = pl.ds(piece * PER * BLK, PER * BLK)
        own = jnp.dot(att[at, :], wo_v[:, pl.ds(mine, 512)], preferred_element_type=F32)
        out_copies[piece].wait_recv()
        out[at, :] = (own + part_in[piece].astype(F32)).astype(BF16)

    for c in tok_copies + nsel_copies + plane_copies + out_copies + list(y_copies.values()):
        c.wait_send()
    for step in ups + downs:
        for c in step:
            c.wait_send()


def body(tokens, norm_gain, w_query, w_key, w_value, q_gain, k_gain, w_out, chosen):
    hbm = pl.BlockSpec(memory_space=pltpu.HBM)
    vmem = pl.BlockSpec(memory_space=pltpu.VMEM)
    dma = pltpu.SemaphoreType.DMA
    mixed, logs = pl.pallas_call(
        kernel,
        out_shape=(
            jax.ShapeDtypeStruct((TOK, 512), BF16),
            jax.ShapeDtypeStruct((HEADS, TOK), F32),
        ),
        in_specs=[hbm] * 9,
        out_specs=(vmem, vmem),
        scratch_shapes=[
            pltpu.VMEM((NB, TOPB), I32),
            pltpu.VMEM((1, 1024), F32),
            pltpu.VMEM((1, HD), F32),
            pltpu.VMEM((1, HD), F32),
            pltpu.VMEM((2, TOK, 512), BF16),
            pltpu.VMEM((TOK, 1024), BF16),
            pltpu.VMEM((1024, 512), BF16),
            pltpu.VMEM((1024, 256), BF16),
            pltpu.VMEM((512, 1024), BF16),
            *[pltpu.VMEM((NB, BLK, 256), BF16) for _ in range(11)],
            pltpu.VMEM((NZ * NY, MOST, BLK, 256), BF16),
            pltpu.VMEM((LANDED, BLK, 256), BF16),
            pltpu.VMEM((NB, 256), I32),
            pltpu.VMEM((len(SERVED), NB, 256), I32),
            pltpu.VMEM((NB, 128), I32),
            pltpu.SMEM((NB, 256), I32),
            pltpu.SMEM((len(SERVED), NB, 256), I32),
            pltpu.SMEM((NB, 128), I32),
            pltpu.VMEM((NB, 8, TOPB * BLK), F32),
            pltpu.VMEM((TOK, 128), F32),
            pltpu.VMEM((TOK, 128), F32),
            pltpu.VMEM((NB, TOK, 128), BF16),
            pltpu.VMEM((TOPB * BLK, 256), BF16),
            pltpu.VMEM((TOK, 512), BF16),
            pltpu.VMEM((NB, TOK, 128), F32),
            pltpu.VMEM((PIECES, PER * BLK, 512), BF16),
            pltpu.VMEM((PIECES, PER * BLK, 512), BF16),
            dma((4,)),
            dma((12,)),
            dma((2 + len(SERVED),)),
            dma((CHUNKS,)), dma((CHUNKS,)),
            dma((len(SERVED),)), dma((len(SERVED),)),
            dma((4 * CHUNKS,)), dma((4 * CHUNKS,)),
            dma((3 * CHUNKS,)), dma((3 * CHUNKS,)),
            dma((NY * CHUNKS,)), dma((NY * CHUNKS,)),
            dma((NZ * NY,)), dma((NZ * NY,)),
            dma((PIECES,)), dma((PIECES,)),
        ],
        compiler_params=pltpu.CompilerParams(
            collective_id=0, has_side_effects=True, vmem_limit_bytes=54700 * 1024
        ),
        name="fused",
    )(
        tokens.reshape(TOK, 512),
        norm_gain.reshape(1, 1024),
        w_query,
        w_key,
        w_value,
        q_gain.reshape(1, HD),
        k_gain.reshape(1, HD),
        w_out,
        chosen.reshape(NB, TOPB),
    )
    return mixed.reshape(1, TOK, 512), logs.reshape(1, HEADS, TOK)


def solution(mesh):
    return jax.shard_map(
        body,
        mesh=mesh,
        in_specs=(
            P("dp", "kv", "tp"), P(), P(None, "tp"), P(None, "tp"), P(None, "tp"),
            P(), P(), P("tp", None), P("dp", "kv", None),
        ),
        out_specs=(P("dp", "kv", "tp"), P("dp", "tp", "kv")),
        check_vma=False,
    )
```

profile of v0, /device:TPU:1, one launch (start us, length us, event | category | flops | bytes accessed | tf_op | source)
XLA Modules:
  0.0 41.7 jit_solution(13088667650103291264)
XLA Ops:
  0.6 0.0 copy-start.1
  0.6 0.0 copy-start
  0.7 0.0 copy-start.2
  0.7 0.0 copy-start.3
  0.7 0.6 %copy-done.1 = s32[1,8,16]{2,1,0:T(8,128)S(1)} copy-done((s32[1,8,16]{2,1,0:T(8,128)S(1)}, s32[1,8,16]{2,1,0:T(8,128)}, u32[]{:S(2)}) %copy-start.1) | copy-done | bytes 536
  1.3 0.0 copy-done
  1.3 0.0 copy-done.2
  1.3 0.0 copy-done.3
  1.3 39.1 %fused.1 = (bf16[256,512]{1,0:T(8,128)(2,1)S(1)}, f32[8,256]{1,0:T(8,128)S(1)}) custom-call(bf16[256,512]{1,0:T(8,128)(2,1)} %bitcast.13, f32[1,1024]{1,0:T(1,128)S(1)} %bitcast.9, bf16[1024,512]{1,0:T(8,128)(2,1)} %wq.1, bf16[1024,128]{1,0:T(8,128)(2,1)} %wk.1, bf16[1024,128]{1,0:T(8,128)(2,1)} %wv.1, f32[1,64]{1,0:T(1,128)S(1)} %bitcast.11, ...), custom_call_target="tpu_custom_call" | custom-call | tf_op jit(solution)/shard_map/fused/pallas_call | solution.py:424
  40.4 0.7 %copy.13 = bf16[1,256,512]{2,1,0:T(8,128)(2,1)} copy(bf16[1,256,512]{2,1,0:T(8,128)(2,1)S(1)} %bitcast.7) | data formatting | bytes 524288
  41.1 0.6 %copy.14 = f32[1,8,256]{2,1,0:T(8,128)} copy(f32[1,8,256]{2,1,0:T(8,128)S(1)} %bitcast.8) | data formatting | bytes 16384
Async XLA Ops:
  0.6 0.7 %copy-start.1 = (s32[1,8,16]{2,1,0:T(8,128)S(1)}, s32[1,8,16]{2,1,0:T(8,128)}, u32[]{:S(2)}) copy-start(s32[1,8,16]{2,1,0:T(8,128)} %param.17) | copy-start | bytes 1540
  0.6 0.7 %copy-start = (f32[1024]{0:T(1024)S(1)}, f32[1024]{0:T(1024)}, u32[]{:S(2)}) copy-start(f32[1024]{0:T(1024)} %param.10) | copy-start | bytes 12292
  0.7 0.7 %copy-start.2 = (f32[64]{0:T(128)S(1)}, f32[64]{0:T(128)}, u32[]{:S(2)}) copy-start(f32[64]{0:T(128)} %param.14) | copy-start | bytes 772
  0.7 0.7 %copy-start.3 = (f32[64]{0:T(128)S(1)}, f32[64]{0:T(128)}, u32[]{:S(2)}) copy-start(f32[64]{0:T(128)} %param.15) | copy-start | bytes 772
where the time goes:
time: 41.8 us; the launch traced here: 41.7 us
  Pallas kernels  39.1 us (94%)
  local copies, waits for them, and re-layouts  1.98 us (5%)
  between operations  0.68 us (2%)
    pallas_call x1, Pallas kernels, body(): pl.pallas_call(kernel, out_shape=(jax.ShapeDtypeStruct((TOK, 512), BF16),...  39.1 us
    unnamed x10, local copies, waits for them, and re-layouts  1.98 us

commit v1 on v0

--- a/solution.py
+++ b/solution.py
@@ -57,8 +57,8 @@
     chosen, gain, qg, kg, tok, hid, wq_v, wkv_v, wo_v,
     c0, c1, c2, c3, c4, c5, c6, c7, p1, p2, p3,
     msg, land, sel_v, nsel_v, ent_v, sel_s, nsel_s, ent_s,
-    upos, bias_t, bias_a, qbd, kvg, att, lsum, part, part_in,
-    small_sem, load_sem, tab_sem, tok_send, tok_recv, nsel_send, nsel_recv,
+    upos, slope, qbd, kvg, att, lsum, part, part_in,
+    small_sem, mine_sem, load_sem, tab_sem, tok_send, tok_recv, nsel_send, nsel_recv,
     up_send, up_recv, dn_send, dn_recv, pln_send, pln_recv, y_send, y_recv, out_send, out_recv,
 ):
     dp = lax.axis_index("dp")
@@ -93,11 +93,16 @@
     ]
     for load in small:
         load.start()
+    tok_loads = [
+        pltpu.make_async_copy(
+            tokens.at[pl.ds(i * STEP, STEP)], tok.at[tp, pl.ds(i * STEP, STEP)], mine_sem.at[i]
+        )
+        for i in range(CHUNKS)
+    ]
     loads = [
-        pltpu.make_async_copy(tokens, tok.at[tp], load_sem.at[0]),
-        pltpu.make_async_copy(wk, wkv_v.at[:, pl.ds(0, 128)], load_sem.at[1]),
-        pltpu.make_async_copy(wv, wkv_v.at[:, pl.ds(128, 128)], load_sem.at[2]),
-        pltpu.make_async_copy(wq, wq_v, load_sem.at[3]),
+        pltpu.make_async_copy(wk, wkv_v.at[:, pl.ds(0, 128)], load_sem.at[0]),
+        pltpu.make_async_copy(wv, wkv_v.at[:, pl.ds(128, 128)], load_sem.at[1]),
+        pltpu.make_async_copy(wq, wq_v, load_sem.at[2]),
     ]
     for p, pair in enumerate(PAIRS):
         for side in range(2):
@@ -105,10 +110,10 @@
                 pltpu.make_async_copy(
                     wo.at[pl.ds(pair[side] * HD, HD), :],
                     wo_v.at[pl.ds(p * 128 + side * HD, HD), :],
-                    load_sem.at[4 + 2 * p + side],
+                    load_sem.at[3 + 2 * p + side],
                 )
             )
-    for load in loads:
+    for load in tok_loads + loads:
         load.start()
 
     small[0].wait()
@@ -162,16 +167,13 @@
     for r in range(NB):
         upos[r] = jnp.broadcast_to(pos[r : r + 1], (8, TOPB * BLK))
 
-    rows = lax.broadcasted_iota(I32, (TOK, 128), 0)
-    head_no = (tp * HEADS + rows // BLK + 1).astype(F32)
-    bias_t[...] = (rows % BLK).astype(F32)
-    bias_a[...] = jnp.exp2(head_no * (-8.0 / 16.0)) * (4.0 / SEQ * LOG2E)
-
+    head_no = (tp * HEADS + lax.broadcasted_iota(I32, (HEADS, 128), 0) + 1).astype(F32)
+    slope[...] = jnp.exp2(head_no * (-8.0 / 16.0)) * (4.0 / SEQ * LOG2E)
     pl.semaphore_wait(barrier, len(peers))
-    loads[0].wait()
     tok_copies = []
     for i in range(CHUNKS):
         at = pl.ds(i * STEP, STEP)
+        tok_loads[i].wait()
         c = remote(tok.at[tp, at], tok.at[tp, at], tok_send.at[i], tok_recv.at[i], partner)
         c.start()
         tok_copies.append(c)
@@ -212,8 +214,8 @@
     g1 = gain[:, 512:1024]
     kgain = jnp.concatenate([kg[...], kg[...]], axis=1)
     qgain = jnp.concatenate([qg[...], qg[...]], axis=1)
+    loads[0].wait()
     loads[1].wait()
-    loads[2].wait()
     plane_copies = []
     for i in range(CHUNKS):
         tok_copies[i].wait_recv()
@@ -310,7 +312,7 @@
     serve(1)
     keep(1, 0)
     keep(7, 0)
-    loads[3].wait()
+    loads[2].wait()
     queries(0, 2, PAIRS[0], PAIRS[2])
     turn(2)
     serve(2)
@@ -334,7 +336,7 @@
     turn(4)
     serve(4)
     keep(4, 0)
-    for load in loads[4:]:
+    for load in loads[3:]:
         load.wait()
     for c in y_copies.values():
         c.wait_recv()
@@ -345,17 +347,22 @@
         raw = lax.dot_general(
             qbd[r], kvg[:, 0:128], (((1,), (1,)), ((), ())), preferred_element_type=F32
         )
-        t = bias_t[...] + ((kv * NB + r) * BLK).astype(F32)
-        a = bias_a[...]
         total = jnp.zeros((TOK, 128), F32)
         probs = []
+        first_key = (kv * NB + r) * BLK
+        later = lax.broadcasted_iota(I32, (BLK, 128), 1) > lax.broadcasted_iota(
+            I32, (BLK, 128), 0
+        )
+        own_lane = lax.broadcasted_iota(I32, (BLK, 128), 1) < BLK
         for i in range(4):
-            u = upos[r, 0:1, 128 * i : 128 * (i + 1)]
+            off = upos[r, :, 128 * i : 128 * (i + 1)] - first_key.astype(F32)
+            factor = jnp.exp2(slope[...] * off)
+            w = jnp.exp2(raw[:, 128 * i : 128 * (i + 1)] * (LOG2E / 8.0)).reshape(
+                HEADS, BLK, 128
+            ) * factor.reshape(HEADS, 1, 128)
             if i == 0:
-                off = jnp.where(u > t, FAR, u - t)
-            else:
-                off = u - t
-            w = jnp.exp2(raw[:, 128 * i : 128 * (i + 1)] * (LOG2E / 8.0) + a * off)
+                w = jnp.where((later & own_lane)[None], 0.0, w)
+            w = w.reshape(TOK, 128)
             total = total + w
             probs.append(w.astype(BF16))
         row_sum = jnp.sum(total, axis=1, keepdims=True)
@@ -400,9 +407,10 @@
         sums = jnp.zeros((TOK, 128), F32)
         for r in range(4):
             sums = jnp.where(lane_q == r * BLK + query, lsum[4 * side + r], sums)
+        ago = (lax.broadcasted_iota(I32, (HEADS, 128), 1) % BLK).astype(F32)
         logs[:, 128 * side : 128 * (side + 1)] = jnp.log(
             jnp.sum(sums.reshape(HEADS, BLK, 128), axis=1)
-        )
+        ) - slope[...] * ago * (1.0 / LOG2E)
     mine = pl.multiple_of(tp * 512, 512)
     for piece in range(PIECES):
         at = pl.ds(piece * PER * BLK, PER * BLK)
@@ -415,6 +423,17 @@
     for step in ups + downs:
         for c in step:
             c.wait_send()
+
+
+def deliver(mixed, logs, mixed_out, logs_out, sem):
+    copies = (
+        pltpu.make_async_copy(mixed, mixed_out, sem.at[0]),
+        pltpu.make_async_copy(logs, logs_out, sem.at[1]),
+    )
+    for c in copies:
+        c.start()
+    for c in copies:
+        c.wait()
 
 
 def body(tokens, norm_gain, w_query, w_key, w_value, q_gain, k_gain, w_out, chosen):
@@ -449,8 +468,7 @@
             pltpu.SMEM((len(SERVED), NB, 256), I32),
             pltpu.SMEM((NB, 128), I32),
             pltpu.VMEM((NB, 8, TOPB * BLK), F32),
-            pltpu.VMEM((TOK, 128), F32),
-            pltpu.VMEM((TOK, 128), F32),
+            pltpu.VMEM((HEADS, 128), F32),
             pltpu.VMEM((NB, TOK, 128), BF16),
             pltpu.VMEM((TOPB * BLK, 256), BF16),
             pltpu.VMEM((TOK, 512), BF16),
@@ -458,7 +476,8 @@
             pltpu.VMEM((PIECES, PER * BLK, 512), BF16),
             pltpu.VMEM((PIECES, PER * BLK, 512), BF16),
             dma((4,)),
-            dma((12,)),
+            dma((CHUNKS,)),
+            dma((11,)),
             dma((2 + len(SERVED),)),
             dma((CHUNKS,)), dma((CHUNKS,)),
             dma((len(SERVED),)), dma((len(SERVED),)),
@@ -483,6 +502,18 @@
         w_out,
         chosen.reshape(NB, TOPB),
     )
+    mixed, logs = pl.pallas_call(
+        deliver,
+        out_shape=(
+            jax.ShapeDtypeStruct((TOK, 512), BF16),
+            jax.ShapeDtypeStruct((HEADS, TOK), F32),
+        ),
+        in_specs=[vmem, vmem],
+        out_specs=(hbm, hbm),
+        scratch_shapes=[dma((2,))],
+        compiler_params=pltpu.CompilerParams(vmem_limit_bytes=8 * 1024 * 1024),
+        name="deliver",
+    )(mixed, logs)
     return mixed.reshape(1, TOK, 512), logs.reshape(1, HEADS, TOK)
 
 

time: 41.8 us -> 41.1 us (0.983)
  local copies, waits for them, and re-layouts: 1.98 us -> 0.68 us
  Pallas kernels: 39.1 us -> 39.6 us
    unnamed x10 -> x8, local copies, waits for them, and re-layouts: 1.98 us -> 0.68 us
    pallas_call x0 -> x1, Pallas kernels: none -> 0.72 us  [body(): pl.pallas_call(deliver, out_shape=(jax.ShapeDtypeStruct((TOK, 512), BF16)...]
where the time goes in v1:
time: 41.1 us; the launch traced here: 41 us
  Pallas kernels  39.6 us (96%)
  local copies, waits for them, and re-layouts  0.68 us (2%)
  between operations  0.67 us (2%)
    pallas_call x1, Pallas kernels, body(): pl.pallas_call(kernel, out_shape=(jax.ShapeDtypeStruct((TOK, 512), BF16),...  38.9 us

profile of v1, /device:TPU:1, one launch (start us, length us, event | category | flops | bytes accessed | tf_op | source)
XLA Modules:
  0.0 41.0 jit_solution(13055657432604402139)
XLA Ops:
  0.6 0.0 copy-start.1
  0.6 0.0 copy-start
  0.7 0.0 copy-start.2
  0.7 0.0 copy-start.3
  0.7 0.6 %copy-done.1 = s32[1,8,16]{2,1,0:T(8,128)S(1)} copy-done((s32[1,8,16]{2,1,0:T(8,128)S(1)}, s32[1,8,16]{2,1,0:T(8,128)}, u32[]{:S(2)}) %copy-start.1) | copy-done | bytes 536
  1.3 0.0 copy-done
  1.3 0.0 copy-done.2
  1.3 0.0 copy-done.3
  1.3 38.9 %fused.1 = (bf16[256,512]{1,0:T(8,128)(2,1)S(1)}, f32[8,256]{1,0:T(8,128)S(1)}) custom-call(bf16[256,512]{1,0:T(8,128)(2,1)} %bitcast.11, f32[1,1024]{1,0:T(1,128)S(1)} %bitcast.7, bf16[1024,512]{1,0:T(8,128)(2,1)} %wq.1, bf16[1024,128]{1,0:T(8,128)(2,1)} %wk.1, bf16[1024,128]{1,0:T(8,128)(2,1)} %wv.1, f32[1,64]{1,0:T(1,128)S(1)} %bitcast.9, ...), custom_call_target="tpu_custom_call" | custom-call | tf_op jit(solution)/shard_map/fused/pallas_call | solution.py:443
  40.3 0.7 %deliver.1 = (bf16[256,512]{1,0:T(8,128)(2,1)}, f32[8,256]{1,0:T(8,128)}) custom-call(bf16[256,512]{1,0:T(8,128)(2,1)S(1)} %get-tuple-element.6.mixed, f32[8,256]{1,0:T(8,128)S(1)} %get-tuple-element.7.logs), custom_call_target="tpu_custom_call" | custom-call | tf_op jit(solution)/shard_map/deliver/pallas_call | solution.py:505
Async XLA Ops:
  0.6 0.7 %copy-start.1 = (s32[1,8,16]{2,1,0:T(8,128)S(1)}, s32[1,8,16]{2,1,0:T(8,128)}, u32[]{:S(2)}) copy-start(s32[1,8,16]{2,1,0:T(8,128)} %param.17) | copy-start | bytes 1540
  0.6 0.7 %copy-start = (f32[1024]{0:T(1024)S(1)}, f32[1024]{0:T(1024)}, u32[]{:S(2)}) copy-start(f32[1024]{0:T(1024)} %param.10) | copy-start | bytes 12292
  0.7 0.7 %copy-start.2 = (f32[64]{0:T(128)S(1)}, f32[64]{0:T(128)}, u32[]{:S(2)}) copy-start(f32[64]{0:T(128)} %param.14) | copy-start | bytes 772
  0.7 0.7 %copy-start.3 = (f32[64]{0:T(128)S(1)}, f32[64]{0:T(128)}, u32[]{:S(2)}) copy-start(f32[64]{0:T(128)} %param.15) | copy-start | bytes 772

commit v2 on v1

--- a/solution.py
+++ b/solution.py
@@ -27,8 +27,11 @@
 LANDED = OWN + NB
 FAR = -1e30
 PAIRS = ((0, 5), (2, 7), (1, 4), (3, 6))
-NEAR = ((0, 1), (0, 2), (0, 3), (1, 0), (-1, 0), (2, 0), (-2, 0))
-SERVED = ((0, 1), (0, 2), (0, 3), (2, 0), (-2, 0), (-1, 0))
+DIRECT = ((7, 1), (7, 2), (7, 3), (2, 2), (6, 2))
+SERVED = ((0, 1), (0, 2), (0, 3)) + tuple(
+    (d if d <= 4 else d - 8, 0) for d in sorted({d for d, _ in DIRECT})
+)
+NEAR = tuple(sorted({(1, 0), (-1, 0), *SERVED, *((-dz, -dy % 4) for dz, dy in SERVED)}))
 CHUNKS = 4
 STEP = TOK // CHUNKS
 PIECES = 2
@@ -253,18 +256,23 @@
         return ((z + dz + NZ) % NZ) * NY + (y + dy + NY) % NY
 
     def send(n, k, source, d, dy):
-        for s in range(MOST):
-            msg[k, s] = picked(nsel_s.at[n], source, d, dy, s)
+        slot = k % NZ
         c = remote(
             msg.at[k], land.at[pl.ds(k * MOST, MOST)],
             y_send.at[k], y_recv.at[k], dev(*SERVED[n]),
         )
-        c.start()
-        y_copies[k] = c
+        wanted = (z + SERVED[n][0] + NZ) % NZ >= slot
+        y_copies[k] = (c, wanted, z >= slot)
+
+        @pl.when(wanted)
+        def _():
+            for s in range(MOST):
+                msg[k, s] = picked(nsel_s.at[n], source, d, dy, s)
+            c.start()
 
     def serve(d):
         for n, dy in ((0, 1), (2, 3), (1, 2)):
-            if not (d in (2, 6) and dy == 2):
+            if (d, dy) not in DIRECT:
                 send(n, dy * NZ + d, device_no(-d, 0), d, 0)
 
     def keep(d, dy):
@@ -319,10 +327,9 @@
     serve(6)
     for c in plane_copies:
         c.wait_recv()
-    for dy in (1, 2, 3):
-        send(5, dy * NZ + 7, device_no(0, -dy), 0, dy)
-    send(3, 2 * NZ + 2, device_no(0, -2), 0, 2)
-    send(4, 2 * NZ + 6, device_no(0, -2), 0, 2)
+    for d, dy in DIRECT:
+        to = SERVED.index((d if d <= 4 else d - 8, 0))
+        send(to, dy * NZ + d, device_no(0, -dy), 0, dy)
     for dy in (1, 2, 3):
         keep(0, dy)
     keep(2, 0)
@@ -338,8 +345,8 @@
     keep(4, 0)
     for load in loads[3:]:
         load.wait()
-    for c in y_copies.values():
-        c.wait_recv()
+    for c, _, awaited in y_copies.values():
+        pl.when(awaited)(c.wait_recv)
 
     def attend(r, carry):
         for e in range(TOPB):
@@ -401,6 +408,14 @@
 
     lax.fori_loop(0, PIECES, do_piece, 0)
     out_copies = [out_copy(piece) for piece in range(PIECES)]
+    for c in tok_copies + nsel_copies + plane_copies:
+        c.wait_send()
+    for c, wanted, _ in y_copies.values():
+        pl.when(wanted)(c.wait_send)
+    for step in ups + downs:
+        for c in step:
+            c.wait_send()
+
     lane_q = lax.broadcasted_iota(I32, (TOK, 128), 1)
     query = lax.broadcasted_iota(I32, (TOK, 128), 0) % BLK
     for side in range(2):
@@ -417,12 +432,8 @@
         own = jnp.dot(att[at, :], wo_v[:, pl.ds(mine, 512)], preferred_element_type=F32)
         out_copies[piece].wait_recv()
         out[at, :] = (own + part_in[piece].astype(F32)).astype(BF16)
-
-    for c in tok_copies + nsel_copies + plane_copies + out_copies + list(y_copies.values()):
+    for c in out_copies:
         c.wait_send()
-    for step in ups + downs:
-        for c in step:
-            c.wait_send()
 
 
 def deliver(mixed, logs, mixed_out, logs_out, sem):

time: 41.1 us -> 36.1 us (0.88)
  the two profiles are of different devices: /device:TPU:1 before, /device:TPU:227 now
where the time goes in v2:
time: 36.1 us; the launch traced here: 35.9 us
  Pallas kernels  34.6 us (96%)
  local copies, waits for them, and re-layouts  0.68 us (2%)
  between operations  0.67 us (2%)
    pallas_call x1, Pallas kernels, body(): pl.pallas_call(kernel, out_shape=(jax.ShapeDtypeStruct((TOK, 512), BF16),...  33.8 us
    pallas_call x1, Pallas kernels, body(): pl.pallas_call(deliver, out_shape=(jax.ShapeDtypeStruct((TOK, 512), BF16)...  0.72 us

profile of v2, /device:TPU:227, one launch (start us, length us, event | category | flops | bytes accessed | tf_op | source)
XLA Modules:
  0.0 35.9 jit_solution(9939393224184476252)
XLA Ops:
  0.6 0.0 copy-start.1
  0.6 0.0 copy-start
  0.7 0.0 copy-start.2
  0.7 0.0 copy-start.3
  0.7 0.6 %copy-done.1 = s32[1,8,16]{2,1,0:T(8,128)S(1)} copy-done((s32[1,8,16]{2,1,0:T(8,128)S(1)}, s32[1,8,16]{2,1,0:T(8,128)}, u32[]{:S(2)}) %copy-start.1) | copy-done | bytes 536
  1.3 0.0 copy-done
  1.3 0.0 copy-done.2
  1.3 0.0 copy-done.3
  1.3 33.8 %fused.1 = (bf16[256,512]{1,0:T(8,128)(2,1)S(1)}, f32[8,256]{1,0:T(8,128)S(1)}) custom-call(bf16[256,512]{1,0:T(8,128)(2,1)} %bitcast.11, f32[1,1024]{1,0:T(1,128)S(1)} %bitcast.7, bf16[1024,512]{1,0:T(8,128)(2,1)} %wq.1, bf16[1024,128]{1,0:T(8,128)(2,1)} %wk.1, bf16[1024,128]{1,0:T(8,128)(2,1)} %wv.1, f32[1,64]{1,0:T(1,128)S(1)} %bitcast.9, ...), custom_call_target="tpu_custom_call" | custom-call | tf_op jit(solution)/shard_map/fused/pallas_call | solution.py:454
  35.2 0.7 %deliver.1 = (bf16[256,512]{1,0:T(8,128)(2,1)}, f32[8,256]{1,0:T(8,128)}) custom-call(bf16[256,512]{1,0:T(8,128)(2,1)S(1)} %get-tuple-element.6.mixed, f32[8,256]{1,0:T(8,128)S(1)} %get-tuple-element.7.logs), custom_call_target="tpu_custom_call" | custom-call | tf_op jit(solution)/shard_map/deliver/pallas_call | solution.py:516
Async XLA Ops:
  0.6 0.7 %copy-start.1 = (s32[1,8,16]{2,1,0:T(8,128)S(1)}, s32[1,8,16]{2,1,0:T(8,128)}, u32[]{:S(2)}) copy-start(s32[1,8,16]{2,1,0:T(8,128)} %param.17) | copy-start | bytes 1540
  0.6 0.7 %copy-start = (f32[1024]{0:T(1024)S(1)}, f32[1024]{0:T(1024)}, u32[]{:S(2)}) copy-start(f32[1024]{0:T(1024)} %param.10) | copy-start | bytes 12292
  0.7 0.7 %copy-start.2 = (f32[64]{0:T(128)S(1)}, f32[64]{0:T(128)}, u32[]{:S(2)}) copy-start(f32[64]{0:T(128)} %param.14) | copy-start | bytes 772
  0.7 0.7 %copy-start.3 = (f32[64]{0:T(128)S(1)}, f32[64]{0:T(128)}, u32[]{:S(2)}) copy-start(f32[64]{0:T(128)} %param.15) | copy-start | bytes 772
